TPU v7x, 32 devices: a whole 2x2x4 slice. The times are simulated.
32 devices in a mesh: ep: 8 (over z, x), tp: 4 (over y, core).
Axes of the slice: x: 2, y: 2, z: 4, core: 2. Of those that a mesh axis runs over, the one named last changes fastest.
Arguments:
- tokens: bfloat16 [4096, 4096], P('ep', 'tp'), may hold values from -100 to 100, as said below
- routes: int32 [4096, 2], P('ep'), may hold values from 0 to 15, all different within a row; in each aligned block of 512 rows (0 to 511, 512 to 1023, ...) at most 128 rows name the same one
- route_weights: float32 [4096, 2], P('ep'), may hold values from 0.1 to 1
- norm_gain: float32 [4096], P('tp'), may hold values from 0.1 to 1.9
- gate_weight: bfloat16 [16, 4096, 512], P('ep', 'tp'), may hold values from -0.09375 to 0.09375
- up_weight: bfloat16 [16, 4096, 512], P('ep', 'tp'), may hold values from -0.09375 to 0.09375
- down_weight: bfloat16 [16, 512, 4096], P('ep', None, 'tp'), may hold values from -0.25 to 0.25
- final_gain: float32 [4096], P('tp'), may hold values from 0.1 to 1.9
Outputs:
- mixed: bfloat16 [4096, 4096], P('ep', 'tp')
Inputs may be any that keep to these rules, and one draw needn't show every extreme that they name: `tokens`: real-valued activations whose features differ in scale. `routes`: each row names 2 different experts; among the 512 rows of one aligned block no expert is named more than 128 times, a bound that some block reaches.
All inputs are finite; a program needn't handle non-finite values.
Results may differ from a plain program's by a relative error of at most 0.018.
Values may be sent and summed in bfloat16 or wider, within the bound.
A program may use at most 64 MiB of HBM per device.

v0:
```python
import jax
import jax.numpy as jnp
from jax import lax
from jax.sharding import PartitionSpec as P

D = 4096
EPSILON = 1e-06


def expert_rows(weights, block):
    w_gate, w_up, w_down = weights
    gate = jnp.einsum("scd,df->scf", block, w_gate, preferred_element_type=jnp.float32)
    upper = jnp.einsum("scd,df->scf", block, w_up, preferred_element_type=jnp.float32)
    gate_sum, upper_sum = (
        lax.psum_scatter(gate.astype(jnp.bfloat16), "tp", scatter_dimension=2, tiled=True).astype(
            jnp.float32
        ),
        lax.psum_scatter(upper.astype(jnp.bfloat16), "tp", scatter_dimension=2, tiled=True).astype(
            jnp.float32
        ),
    )
    share = (jax.nn.silu(gate_sum) * upper_sum).astype(jnp.bfloat16)
    hidden = lax.all_gather(share, "tp", axis=2, tiled=True)
    return jnp.einsum("scf,fd->scd", hidden, w_down, preferred_element_type=jnp.float32).astype(
        jnp.bfloat16
    )


def serve_single(weights, block):
    return lax.all_to_all(
        expert_rows(weights, block), "ep", split_axis=0, concat_axis=0, tiled=True
    )


def body(tokens, routes, route_weights, norm_gain, gate_weight, up_weight, down_weight, final_gain):
    ep_count = lax.axis_size("ep")
    local_count = gate_weight.shape[0]
    experts = ep_count * local_count
    tok_rows = tokens.shape[0]
    top_count = routes.shape[1]
    capacity = 4 * tok_rows // experts
    values = tokens.astype(jnp.float32)
    squares = lax.psum(jnp.sum(values * values, axis=-1), "tp")
    normed = (values * lax.rsqrt(squares / D + EPSILON)[:, None] * norm_gain).astype(jnp.bfloat16)
    chosen = routes.reshape(-1)
    onehot = (chosen[:, None] == jnp.arange(experts, dtype=jnp.int32)[None, :]).astype(jnp.int32)
    slots = jnp.sum((jnp.cumsum(onehot, axis=0) - onehot) * onehot, axis=1)
    target = chosen * capacity + slots
    owners = jnp.arange(tok_rows * top_count, dtype=jnp.int32) // top_count
    table = jnp.full((experts * capacity,), tok_rows, jnp.int32).at[target].set(owners)
    padded = jnp.concatenate([normed, jnp.zeros((1, normed.shape[1]), jnp.bfloat16)], axis=0)
    outgoing = padded[table].reshape(ep_count, local_count, capacity, normed.shape[1])
    weight_list = [
        (gate_weight[member], up_weight[member], down_weight[member])
        for member in range(local_count)
    ]
    pieces = []
    for member in range(local_count):
        pieces.append(
            serve_single(
                weight_list[member],
                lax.all_to_all(outgoing[:, member], "ep", split_axis=0, concat_axis=0, tiled=True),
            )
        )
    arrived = jnp.stack(pieces, axis=1)
    returned = arrived.reshape(experts * capacity, normed.shape[1])
    position = target.reshape(tok_rows, top_count)
    combined = jnp.zeros((tok_rows, normed.shape[1]), jnp.float32)
    for which in range(top_count):
        combined = combined + route_weights[:, which : which + 1] * returned[
            position[:, which]
        ].astype(jnp.float32)
    closing = lax.psum(jnp.sum(combined * combined, axis=-1), "tp")
    return (combined * lax.rsqrt(closing / D + EPSILON)[:, None] * final_gain).astype(jnp.bfloat16)


def solution(mesh):
    in_specs = (
        P("ep", "tp"),
        P("ep", None),
        P("ep", None),
        P("tp"),
        P("ep", "tp", None),
        P("ep", "tp", None),
        P("ep", None, "tp"),
        P("tp"),
    )
    out_specs = P("ep", "tp")
    return jax.shard_map(body, mesh=mesh, in_specs=in_specs, out_specs=out_specs, check_vma=False)
```

profile of v0, /device:TPU:0, one launch (start us, length us, event | category | flops | bytes accessed | tf_op | source)
XLA Modules:
  0.0 332.4 jit_solution(4399818030590045528)
XLA Ops:
  6.5 0.9 copy.27
  7.5 0.2 eq.29
  7.6 0.2 eq.25
  7.8 1.5 fusion
  9.3 8.4 %psum.14 = f32[512]{0:T(512)S(1)} all-reduce(f32[512]{0:T(512)S(1)} %fusion), channel_id=1, replica_groups=mesh['ep'=8,'tp'=4] {'tp'}, use_global_device_ids=true, to_apply=%region_1.0 | all-reduce | flops 512 | bytes 4096 | tf_op jit(solution)/shard_map/psum | solution.py:43
  17.7 4.5 %reduce-window.6 = s32[16,8,128]{2,1,0:T(8,128)S(1)} reduce-window(s32[16,8,128]{2,1,0:T(8,128)S(1)} %fusion.30, s32[]{:T(128)} %constant.41.clone.1), window={size=1x1x128 pad=0_0x0_0x127_0}, to_apply=%region_2.0 | reduce-window | flops 2080768 | bytes 131076 | tf_op jit(solution)/shard_map/reduce-window
  22.2 0.1 slice.62
  22.3 0.1 copy.30
  22.5 0.1 copy.31
  22.6 0.1 broadcast_add_fusion
  22.7 0.2 reduce_sum.34
  22.9 0.2 mul.100
  23.1 4.3 %scatter_custom_fusion = s32[2048]{0:T(1024)S(1)} fusion(s32[1024]{0:T(1024)S(1)} %bitcast.128, s32[1024]{0:T(1024)S(1)} %add_select_fusion, s32[]{:T(128)} %constant.39.clone.1), kind=kCustom, calls=%fused_computation.75 | custom fusion | bytes 8196 | tf_op jit(solution)/shard_map/scatter | solution.py:50
  27.5 0.3 fusion.2
  27.8 0.1 concatenate.3
  27.9 9.7 %gather_fusion = bf16[2048,1024]{1,0:T(8,128)(2,1)} fusion(bf16[513,1024]{1,0:T(8,128)(2,1)S(1)} %concatenate.3, s32[2048]{0:T(1024)S(1)} %fusion.31), kind=kCustom, calls=%fused_computation | custom fusion | bytes 8396800 | tf_op jit(solution)/shard_map/gather | solution.py:52
  37.6 4.0 %slice_bitcast_fusion.1 = (bf16[8,128,1024]{2,1,0:T(8,128)(2,1)}, bf16[8,128,1024]{2,1,0:T(8,128)(2,1)S(1)}) fusion(bf16[8,2,128,1024]{3,2,1,0:T(8,128)(2,1)} %bitcast.103), kind=kLoop, calls=%fused_computation.11 | loop fusion | bytes 8388608 | tf_op jit(solution)/shard_map/squeeze | solution.py:62
  41.7 52.7 %all_to_all.20 = bf16[8,128,1024]{2,1,0:T(8,128)(2,1)S(1)} all-to-all(bf16[8,128,1024]{2,1,0:T(8,128)(2,1)S(1)} %get-tuple-element.8), channel_id=1, replica_groups=mesh['ep'=8,'tp'=4] {'ep'}, dimensions={0} | all-to-all | bytes 4194304 | tf_op jit(solution)/shard_map/all_to_all | solution.py:62
  94.4 2.2 convolution_convert_fusion.2
  96.6 1.7 copy.41
  98.3 1.2 copy.59
  99.6 4.4 %all-to-all-start = ((bf16[8,128,1024]{2,1,0:T(8,128)(2,1)}), bf16[8,128,1024]{2,1,0:T(8,128)(2,1)}, u32[]{:S(2)}, u32[]{:S(2)}) async-start(bf16[8,128,1024]{2,1,0:T(8,128)(2,1)} %get-tuple-element.7), calls=%async_computation | async-start | bytes 4194304 | tf_op jit(solution)/shard_map/all_to_all | solution.py:62
  104.0 0.0 reduce-scatter.17.cloned.1.call-start
  104.0 3.4 %convolution_convert_fusion.3 = bf16[8,128,512]{2,1,0:T(8,128)(2,1)} fusion(bf16[8,128,1024]{2,1,0:T(8,128)(2,1)S(1)} %all_to_all.20, bf16[2,1024,512]{2,1,0:T(8,128)(2,1)} %param.12), kind=kOutput, calls=%fused_computation.18 | convolution fusion | flops 1074266112 | bytes 4194304 | tf_op jit(solution)/shard_map/scd,df->scf/dot_general | solution.py:12
  107.5 1.7 copy.39
  109.2 1.2 copy.60
  110.5 0.0 all-gather.5.cloned.1.call-start
  110.5 13.1 %reduce-scatter.19.cloned.1.call-done = bf16[128,1024]{1,0:T(8,128)(2,1)} async-done(((bf16[512,1024]{1,0:T(8,128)(2,1)}), bf16[128,1024]{1,0:T(8,128)(2,1)}) %reduce-scatter.19.cloned.1.call-update) | async-done | bytes 262160
  123.6 1.0 copy.53
  124.6 0.2 copy.42
  124.9 26.1 %reduce-scatter.17.cloned.1.call-done = bf16[128,1024]{1,0:T(8,128)(2,1)} async-done(((bf16[512,1024]{1,0:T(8,128)(2,1)}), bf16[128,1024]{1,0:T(8,128)(2,1)}) %reduce-scatter.17.cloned.1.call-update) | async-done | bytes 262160
  151.0 1.0 copy.51
  152.0 0.2 copy.40
  152.2 0.9 fusion.23
  153.1 0.0 reduce-scatter.15.cloned.1.call-start
  153.2 3.1 convolution_convert_fusion.4
  156.3 0.8 copy.37
  157.1 1.2 copy.61
  158.4 3.2 convolution_convert_fusion.5
  161.6 0.8 copy.35
  162.4 1.3 copy.62
  163.7 6.5 %all-gather.5.cloned.1.call-done = bf16[8,128,512]{2,1,0:T(8,128)(2,1)} async-done(((bf16[8,128,128]{2,1,0:T(8,128)(2,1)}), bf16[8,128,512]{2,1,0:T(8,128)(2,1)}) %all-gather.5.cloned.1.call-update) | async-done | bytes 1048592 | tf_op jit(solution)/shard_map/all_gather | solution.py:23
  170.1 3.8 %convolution_convert_fusion = bf16[8,128,1024]{2,1,0:T(8,128)(2,1)} fusion(bf16[8,128,512]{2,1,0:T(8,128)(2,1)} %all-gather.5.cloned.1.call-done, bf16[2,512,1024]{2,1,0:T(8,128)(2,1)S(1)} %copy-done.5), kind=kOutput, calls=%fused_computation.15 | convolution fusion | flops 1074790400 | bytes 4194304 | tf_op jit(solution)/shard_map/scf,fd->scd/dot_general | solution.py:24
  174.0 5.5 %all-to-all-start.3 = ((bf16[8,128,1024]{2,1,0:T(8,128)(2,1)}), bf16[8,128,1024]{2,1,0:T(8,128)(2,1)S(1)}, u32[]{:S(2)}, u32[]{:S(2)}) async-start(bf16[8,128,1024]{2,1,0:T(8,128)(2,1)} %convolution_convert_fusion), calls=%async_computation.3 | async-start | bytes 4194304 | tf_op jit(solution)/shard_map/all_to_all | solution.py:30
  179.5 0.2 all-gather.3.cloned.1.call-start
  179.7 17.6 %reduce-scatter.15.cloned.1.call-done = bf16[128,1024]{1,0:T(8,128)(2,1)} async-done(((bf16[512,1024]{1,0:T(8,128)(2,1)}), bf16[128,1024]{1,0:T(8,128)(2,1)}) %reduce-scatter.15.cloned.1.call-update) | async-done | bytes 262160
  197.3 1.0 copy.49
  198.3 0.2 copy.38
  198.6 26.0 %reduce-scatter.13.cloned.1.call-done = bf16[128,1024]{1,0:T(8,128)(2,1)} async-done(((bf16[512,1024]{1,0:T(8,128)(2,1)}), bf16[128,1024]{1,0:T(8,128)(2,1)}) %reduce-scatter.13.cloned.1.call-update) | async-done | bytes 262160
  224.5 1.0 copy.47
  225.5 0.2 copy.36
  225.8 0.9 fusion.24
  226.7 17.0 %all-gather.3.cloned.1.call-done = bf16[8,128,512]{2,1,0:T(8,128)(2,1)} async-done(((bf16[8,128,128]{2,1,0:T(8,128)(2,1)}), bf16[8,128,512]{2,1,0:T(8,128)(2,1)}) %all-gather.3.cloned.1.call-update) | async-done | bytes 1048592 | tf_op jit(solution)/shard_map/all_gather | solution.py:23
  243.6 4.1 %convolution_convert_fusion.1 = bf16[8,128,1024]{2,1,0:T(8,128)(2,1)} fusion(bf16[8,128,512]{2,1,0:T(8,128)(2,1)} %all-gather.3.cloned.1.call-done, bf16[2,512,1024]{2,1,0:T(8,128)(2,1)} %param.14), kind=kOutput, calls=%fused_computation.16 | convolution fusion | flops 1074790400 | bytes 4194304 | tf_op jit(solution)/shard_map/scf,fd->scd/dot_general | solution.py:24
  247.7 5.6 %all-to-all-start.1 = ((bf16[8,128,1024]{2,1,0:T(8,128)(2,1)}), bf16[8,128,1024]{2,1,0:T(8,128)(2,1)}, u32[]{:S(2)}, u32[]{:S(2)}) async-start(bf16[8,128,1024]{2,1,0:T(8,128)(2,1)} %convolution_convert_fusion.1), calls=%async_computation.1 | async-start | bytes 4194304 | tf_op jit(solution)/shard_map/all_to_all | solution.py:30
  253.4 0.3 fusion.25
  253.7 48.4 %all-to-all-done.1 = bf16[8,128,1024]{2,1,0:T(8,128)(2,1)} async-done(((bf16[8,128,1024]{2,1,0:T(8,128)(2,1)}), bf16[8,128,1024]{2,1,0:T(8,128)(2,1)}, u32[]{:S(2)}, u32[]{:S(2)}) %all-to-all-start.1) | async-done | bytes 2097184 | tf_op jit(solution)/shard_map/all_to_all | solution.py:30
  302.1 2.0 pad_maximum_fusion
  304.1 2.4 copy.34
  306.5 5.5 %gather_fusion.2 = bf16[512,1024]{1,0:T(8,128)(2,1)S(1)} fusion(bf16[2048,1024]{1,0:T(8,128)(2,1)} %bitcast.101, s32[1024]{0:T(1024)S(1)} %get-tuple-element.13), kind=kCustom, calls=%fused_computation.2 | custom fusion | bytes 2099200 | tf_op jit(solution)/shard_map/gather | solution.py:70
  311.9 5.5 %gather_fusion.1 = bf16[512,1024]{1,0:T(8,128)(2,1)S(1)} fusion(bf16[2048,1024]{1,0:T(8,128)(2,1)} %bitcast.102, s32[1024]{0:T(1024)S(1)} %get-tuple-element.14), kind=kCustom, calls=%fused_computation.1 | custom fusion | bytes 2099200 | tf_op jit(solution)/shard_map/gather | solution.py:70
  317.4 0.6 multiply_reduce_fusion
  318.0 5.9 %psum.15 = f32[512]{0:T(512)S(1)} all-reduce(f32[512]{0:T(512)S(1)} %multiply_reduce_fusion), channel_id=1, replica_groups=mesh['ep'=8,'tp'=4] {'tp'}, use_global_device_ids=true, to_apply=%region_11.12 | all-reduce | flops 512 | bytes 4096 | tf_op jit(solution)/shard_map/psum | solution.py:73
  324.0 1.6 multiply_convert_fusion
  (34 shorter events, 0.3 us)
Async XLA Ops:
  6.5 21.0 %copy-start = (bf16[512,1024]{1,0:T(8,128)(2,1)S(1)}, bf16[512,1024]{1,0:T(8,128)(2,1)}, u32[]{:S(2)}) copy-start(bf16[512,1024]{1,0:T(8,128)(2,1)} %param.8) | copy-start | bytes 3145732
  6.5 21.0 %copy-start.1 = (f32[1024]{0:T(1024)S(1)}, f32[1024]{0:T(1024)}, u32[]{:S(2)}) copy-start(f32[1024]{0:T(1024)} %param.11) | copy-start | bytes 12292
  6.5 117.1 %reduce-scatter.19.cloned.1.call-start = ((), (), s32[]{:S(2)}) async-start(), calls=%async_computation.13 | async-start | bytes 1310720
  41.6 52.7 %copy-start.4 = (bf16[2,1024,512]{2,1,0:T(8,128)(2,1)S(1)}, bf16[2,1024,512]{2,1,0:T(8,128)(2,1)}, u32[]{:S(2)}) copy-start(bf16[2,1024,512]{2,1,0:T(8,128)(2,1)} %param.13) | copy-start | bytes 6291460
  99.6 53.6 %all-to-all-start = ((bf16[8,128,1024]{2,1,0:T(8,128)(2,1)}), bf16[8,128,1024]{2,1,0:T(8,128)(2,1)}, u32[]{:S(2)}, u32[]{:S(2)}) async-start(bf16[8,128,1024]{2,1,0:T(8,128)(2,1)} %get-tuple-element.7), calls=%async_computation | async-start | bytes 4194304 | tf_op jit(solution)/shard_map/all_to_all | solution.py:62
  104.0 47.0 %reduce-scatter.17.cloned.1.call-start = ((), (), s32[]{:S(2)}) async-start(), calls=%async_computation.12 | async-start | bytes 1310720
  110.5 59.6 %all-gather.5.cloned.1.call-start = ((), (), s32[]{:S(2)}) async-start(), calls=%async_computation.9 | async-start | bytes 1310720 | tf_op jit(solution)/shard_map/all_gather | solution.py:23
  153.1 44.2 %reduce-scatter.15.cloned.1.call-start = ((), (), s32[]{:S(2)}) async-start(), calls=%async_computation.11 | async-start | bytes 1310720
  158.3 66.2 %reduce-scatter.13.cloned.1.call-start = ((), (), s32[]{:S(2)}) async-start(), calls=%async_computation.10 | async-start | bytes 1310720
  162.4 7.8 %copy-start.5 = (bf16[2,512,1024]{2,1,0:T(8,128)(2,1)S(1)}, bf16[2,512,1024]{2,1,0:T(8,128)(2,1)}, u32[]{:S(2)}) copy-start(bf16[2,512,1024]{2,1,0:T(8,128)(2,1)} %param.14) | copy-start | bytes 6291460
  174.0 73.8 %all-to-all-start.3 = ((bf16[8,128,1024]{2,1,0:T(8,128)(2,1)}), bf16[8,128,1024]{2,1,0:T(8,128)(2,1)S(1)}, u32[]{:S(2)}, u32[]{:S(2)}) async-start(bf16[8,128,1024]{2,1,0:T(8,128)(2,1)} %convolution_convert_fusion), calls=%async_computation.3 | async-start | bytes 4194304 | tf_op jit(solution)/shard_map/all_to_all | solution.py:30
  179.5 64.2 %all-gather.3.cloned.1.call-start = ((), (), s32[]{:S(2)}) async-start(), calls=%async_computation.8 | async-start | bytes 1310720 | tf_op jit(solution)/shard_map/all_gather | solution.py:23
  247.7 6.0 %copy-start.3 = (f32[512,2]{0,1:T(2,128)S(1)}, f32[512,2]{0,1:T(2,128)}, u32[]{:S(2)}) copy-start(f32[512,2]{0,1:T(2,128)} %param.10) | copy-start | bytes 12292
  247.7 54.4 %all-to-all-start.1 = ((bf16[8,128,1024]{2,1,0:T(8,128)(2,1)}), bf16[8,128,1024]{2,1,0:T(8,128)(2,1)}, u32[]{:S(2)}, u32[]{:S(2)}) async-start(bf16[8,128,1024]{2,1,0:T(8,128)(2,1)} %convolution_convert_fusion.1), calls=%async_computation.1 | async-start | bytes 4194304 | tf_op jit(solution)/shard_map/all_to_all | solution.py:30
  317.4 6.6 %copy-start.2 = (f32[1024]{0:T(1024)S(1)}, f32[1024]{0:T(1024)}, u32[]{:S(2)}) copy-start(f32[1024]{0:T(1024)} %param.15) | copy-start | bytes 12292
Sparse Core Ops, SparseCore 0:
  99.7 23.8 reduce-scatter.18
  126.1 24.8 reduce-scatter.16
  153.3 16.8 all-gather.4
  172.5 24.7 reduce-scatter.14
  199.7 24.7 reduce-scatter.12
  226.8 16.8 all-gather.2
where the time goes:
time: 333 us; the launch traced here: 332 us
  waiting for transfers between devices  155 us (47%)
  blocking collectives  67.1 us (20%)
  local copies, waits for them, and re-layouts  48.2 us (14%)
  matrix products  19.9 us (6%)
  starting transfers between devices  15.9 us (5%)
  between operations  13.8 us (4%)
  other arithmetic  12.8 us (4%)
    unnamed x10, waiting for transfers between devices  82.9 us
    all_to_all x1, blocking collectives, body(): lax.all_to_all(outgoing[:, member], 'ep', split_axis=0, concat_axis=0, ti...  52.7 us
    all_to_all x2, waiting for transfers between devices, serve_single(): lax.all_to_all(expert_rows(weights, block), 'ep', split_axis=0, concat_ax...  48.4 us
    all_gather x2, waiting for transfers between devices, expert_rows(): hidden = lax.all_gather(share, 'tp', axis=2, tiled=True)  23.4 us
    unnamed x29, local copies, waits for them, and re-layouts  15.8 us
    all_to_all x2, starting transfers between devices, serve_single(): lax.all_to_all(expert_rows(weights, block), 'ep', split_axis=0, concat_ax...  11.2 us
    gather x2, local copies, waits for them, and re-layouts, body(): returned[position[:, which]].astype(jnp.float32)  10.9 us
    gather x1, local copies, waits for them, and re-layouts, body(): padded[table].reshape(ep_count, local_count, capacity, normed.shape[1])  9.7 us
  transfers between devices with their start and end apart: 9, of which 7 were waited for; matrix products, arithmetic and copies ran while one was open for 10% of the time, Pallas kernels for 0%

commit v1 on v0

--- a/solution.py
+++ b/solution.py
@@ -5,6 +5,21 @@
 
 D = 4096
 EPSILON = 1e-06
+
+
+def tracks_treat(content, axis_k):
+    mesh_name = "tp"
+    q_n = lax.axis_size(mesh_name)
+    u1 = sorted(((idx, (idx + 1) % q_n) for idx in range(q_n)))
+    z = content
+    xs_all = [z]
+    for pp in range(1, q_n):
+        z = lax.ppermute(z, mesh_name, u1)
+        xs_all.insert(0, z)
+    v_next = jnp.concatenate(xs_all, axis=axis_k)
+    heard = lax.axis_index(mesh_name)
+    wide_out = heard + 1
+    return jnp.roll(v_next, wide_out * content.shape[axis_k], axis=axis_k)
 
 
 def expert_rows(weights, block):
@@ -20,7 +35,7 @@
         ),
     )
     share = (jax.nn.silu(gate_sum) * upper_sum).astype(jnp.bfloat16)
-    hidden = lax.all_gather(share, "tp", axis=2, tiled=True)
+    hidden = tracks_treat(share, 2)
     return jnp.einsum("scf,fd->scd", hidden, w_down, preferred_element_type=jnp.float32).astype(
         jnp.bfloat16
     )

time: 333 us -> 320 us (0.961)
  waiting for transfers between devices: 155 us -> 145 us
  starting transfers between devices: 15.9 us -> 12.5 us
    unnamed x10 -> x8, waiting for transfers between devices: 82.9 us -> 18.6 us
    all_to_all x1, waiting for transfers between devices: 0.01 us -> 40.7 us  [body(): lax.all_to_all(outgoing[:, member], 'ep', split_axis=0, concat_axis=0, ti...]
    ppermute x0 -> x6, waiting for transfers between devices: none -> 34.8 us  [tracks_treat(): z = lax.ppermute(z, mesh_name, u1)]
    all_gather x2 -> x0, waiting for transfers between devices: 23.4 us -> none  [expert_rows(): hidden = lax.all_gather(share, 'tp', axis=2, tiled=True)]
    unnamed x29 -> x27, local copies, waits for them, and re-layouts: 15.8 us -> 15.8 us
  transfers between devices with their start and end apart: 9 -> 13, of which waited for: 7 -> 10; matrix products, arithmetic and copies ran while one was open for 10% -> 10% of each run, Pallas kernels for 0% -> 0%
where the time goes in v1:
time: 320 us; the launch traced here: 319 us
  waiting for transfers between devices  145 us (45%)
  blocking collectives  66.8 us (21%)
  local copies, waits for them, and re-layouts  48.1 us (15%)
  matrix products  20.9 us (7%)
  between operations  13.5 us (4%)
  starting transfers between devices  12.5 us (4%)
  other arithmetic  11.4 us (4%)
    all_to_all x1, blocking collectives, body(): lax.all_to_all(outgoing[:, member], 'ep', split_axis=0, concat_axis=0, ti...  52.7 us
    all_to_all x2, waiting for transfers between devices, serve_single(): lax.all_to_all(expert_rows(weights, block), 'ep', split_axis=0, concat_ax...  51.4 us
    all_to_all x1, waiting for transfers between devices, body(): lax.all_to_all(outgoing[:, member], 'ep', split_axis=0, concat_axis=0, ti...  40.7 us
    ppermute x6, waiting for transfers between devices, tracks_treat(): z = lax.ppermute(z, mesh_name, u1)  34.8 us
    unnamed x8, waiting for transfers between devices  18.6 us
    unnamed x27, local copies, waits for them, and re-layouts  15.8 us
    gather x2, local copies, waits for them, and re-layouts, body(): returned[position[:, which]].astype(jnp.float32)  10.9 us
    gather x1, local copies, waits for them, and re-layouts, body(): padded[table].reshape(ep_count, local_count, capacity, normed.shape[1])  9.67 us
  transfers between devices with their start and end apart: 13, of which 10 were waited for; matrix products, arithmetic and copies ran while one was open for 10% of the time, Pallas kernels for 0%

profile of v1, /device:TPU:0, one launch (start us, length us, event | category | flops | bytes accessed | tf_op | source)
XLA Modules:
  0.0 318.7 jit_solution(8232916756196982892)
XLA Ops:
  6.5 0.9 copy.27
  7.5 0.2 eq.31
  7.6 0.2 eq.27
  7.8 1.5 fusion
  9.3 8.4 %psum.14 = f32[512]{0:T(512)S(1)} all-reduce(f32[512]{0:T(512)S(1)} %fusion), channel_id=1, replica_groups=mesh['ep'=8,'tp'=4] {'tp'}, use_global_device_ids=true, to_apply=%region_1.0 | all-reduce | flops 512 | bytes 4096 | tf_op jit(solution)/shard_map/psum | solution.py:58
  17.7 4.5 %reduce-window.6 = s32[16,8,128]{2,1,0:T(8,128)S(1)} reduce-window(s32[16,8,128]{2,1,0:T(8,128)S(1)} %fusion.48, s32[]{:T(128)} %constant.63.clone.1), window={size=1x1x128 pad=0_0x0_0x127_0}, to_apply=%region_2.0 | reduce-window | flops 2080768 | bytes 131076 | tf_op jit(solution)/shard_map/reduce-window
  22.2 0.1 slice.62
  22.3 0.1 copy.30
  22.5 0.1 copy.31
  22.6 0.1 broadcast_add_fusion
  22.7 0.2 reduce_sum.34
  22.9 0.2 mul.104
  23.1 4.3 %scatter_custom_fusion = s32[2048]{0:T(1024)S(1)} fusion(s32[1024]{0:T(1024)S(1)} %bitcast.126, s32[1024]{0:T(1024)S(1)} %add_select_fusion, s32[]{:T(128)} %constant.61.clone.1), kind=kCustom, calls=%fused_computation.107 | custom fusion | bytes 8196 | tf_op jit(solution)/shard_map/scatter | solution.py:65
  27.5 0.3 fusion.2
  27.8 0.1 concatenate.12
  27.9 9.7 %gather_fusion = bf16[2048,1024]{1,0:T(8,128)(2,1)} fusion(bf16[513,1024]{1,0:T(8,128)(2,1)S(1)} %concatenate.12, s32[2048]{0:T(1024)S(1)} %fusion.49), kind=kCustom, calls=%fused_computation | custom fusion | bytes 8396800 | tf_op jit(solution)/shard_map/gather | solution.py:67
  37.6 4.0 %slice_bitcast_fusion.1 = (bf16[8,128,1024]{2,1,0:T(8,128)(2,1)}, bf16[8,128,1024]{2,1,0:T(8,128)(2,1)S(1)}) fusion(bf16[8,2,128,1024]{3,2,1,0:T(8,128)(2,1)} %bitcast.101), kind=kLoop, calls=%fused_computation.11 | loop fusion | bytes 8388608 | tf_op jit(solution)/shard_map/squeeze | solution.py:77
  41.6 52.7 %all_to_all.20 = bf16[8,128,1024]{2,1,0:T(8,128)(2,1)S(1)} all-to-all(bf16[8,128,1024]{2,1,0:T(8,128)(2,1)S(1)} %get-tuple-element.9), channel_id=1, replica_groups=mesh['ep'=8,'tp'=4] {'ep'}, dimensions={0} | all-to-all | bytes 4194304 | tf_op jit(solution)/shard_map/all_to_all | solution.py:77
  94.3 2.2 convolution_convert_fusion.2
  96.5 1.7 copy.41
  98.3 1.2 copy.59
  99.5 4.4 %all-to-all-start = ((bf16[8,128,1024]{2,1,0:T(8,128)(2,1)}), bf16[8,128,1024]{2,1,0:T(8,128)(2,1)}, u32[]{:S(2)}, u32[]{:S(2)}) async-start(bf16[8,128,1024]{2,1,0:T(8,128)(2,1)} %get-tuple-element.8), calls=%async_computation | async-start | bytes 4194304 | tf_op jit(solution)/shard_map/all_to_all | solution.py:77
  104.0 3.5 %convolution_convert_fusion.3 = bf16[8,128,512]{2,1,0:T(8,128)(2,1)} fusion(bf16[8,128,1024]{2,1,0:T(8,128)(2,1)S(1)} %all_to_all.20, bf16[2,1024,512]{2,1,0:T(8,128)(2,1)} %param.14), kind=kOutput, calls=%fused_computation.34 | convolution fusion | flops 1074266112 | bytes 4194304 | tf_op jit(solution)/shard_map/scd,df->scf/dot_general | solution.py:27
  107.4 1.7 copy.39
  109.1 1.3 copy.60
  110.5 40.7 %all-to-all-done = bf16[8,128,1024]{2,1,0:T(8,128)(2,1)} async-done(((bf16[8,128,1024]{2,1,0:T(8,128)(2,1)}), bf16[8,128,1024]{2,1,0:T(8,128)(2,1)}, u32[]{:S(2)}, u32[]{:S(2)}) %all-to-all-start) | async-done | bytes 2097184 | tf_op jit(solution)/shard_map/all_to_all | solution.py:77
  151.1 3.1 convolution_convert_fusion.4
  154.2 0.8 copy.37
  155.0 1.3 copy.61
  156.4 1.0 copy.53
  157.4 0.2 copy.42
  157.6 1.0 copy.51
  158.6 0.2 copy.40
  158.9 0.2 fusion.41
  159.0 0.1 collective-permute-start.3
  159.1 5.8 %collective-permute-done.3 = bf16[8,128,128]{2,1,0:T(8,128)(2,1)S(1)} collective-permute-done((bf16[8,128,128]{2,1,0:T(8,128)(2,1)S(1)}, bf16[8,128,128]{2,1,0:T(8,128)(2,1)S(1)}, u32[]{:S(2)}, u32[]{:S(2)}) %collective-permute-start.3) | collective-permute-done | bytes 262176 | tf_op jit(solution)/shard_map/ppermute | solution.py:17
  164.9 5.8 %collective-permute-done.4 = bf16[8,128,128]{2,1,0:T(8,128)(2,1)S(1)} collective-permute-done((bf16[8,128,128]{2,1,0:T(8,128)(2,1)S(1)}, bf16[8,128,128]{2,1,0:T(8,128)(2,1)S(1)}, u32[]{:S(2)}, u32[]{:S(2)}) %collective-permute-start.4) | collective-permute-done | bytes 262176 | tf_op jit(solution)/shard_map/ppermute | solution.py:17
  170.7 3.3 %convolution_convert_fusion.5 = bf16[8,128,512]{2,1,0:T(8,128)(2,1)S(1)} fusion(bf16[8,128,1024]{2,1,0:T(8,128)(2,1)} %all-to-all-done, bf16[2,1024,512]{2,1,0:T(8,128)(2,1)} %param.14), kind=kOutput, calls=%fused_computation.36 | convolution fusion | flops 1074266112 | bytes 4194304 | tf_op jit(solution)/shard_map/scd,df->scf/dot_general | solution.py:27
  174.0 0.8 copy.35
  174.7 1.2 copy.62
  176.0 5.8 %collective-permute-done.5 = bf16[8,128,128]{2,1,0:T(8,128)(2,1)S(1)} collective-permute-done((bf16[8,128,128]{2,1,0:T(8,128)(2,1)S(1)}, bf16[8,128,128]{2,1,0:T(8,128)(2,1)S(1)}, u32[]{:S(2)}, u32[]{:S(2)}) %collective-permute-start.5) | collective-permute-done | bytes 262176 | tf_op jit(solution)/shard_map/ppermute | solution.py:17
  181.8 4.5 %convolution_convert_fusion = bf16[8,128,1024]{2,1,0:T(8,128)(2,1)} fusion(s32[]{:T(128)S(6)} %select_n.44, bf16[8,128,128]{2,1,0:T(8,128)(2,1)S(1)} %collective-permute-done.5, bf16[8,128,128]{2,1,0:T(8,128)(2,1)S(1)} %collective-permute-done.4, bf16[8,128,128]{2,1,0:T(8,128)(2,1)S(1)} %collective-permute-done.3, bf16[8,128,128]{2,1,0:T(8,128)(2,1)S(1)} %fusion.41, ...), kind=kOutput, calls=%fused_computation.31 | convolution fusion | flops 1083179008 | bytes 4194308 | tf_op jit(solution)/shard_map/scf,fd->scd/dot_general | solution.py:39
  186.3 3.6 %all-to-all-start.3 = ((bf16[8,128,1024]{2,1,0:T(8,128)(2,1)}), bf16[8,128,1024]{2,1,0:T(8,128)(2,1)S(1)}, u32[]{:S(2)}, u32[]{:S(2)}) async-start(bf16[8,128,1024]{2,1,0:T(8,128)(2,1)} %convolution_convert_fusion), calls=%async_computation.3 | async-start | bytes 4194304 | tf_op jit(solution)/shard_map/all_to_all | solution.py:45
  189.9 1.0 copy.49
  190.9 0.2 copy.38
  191.2 18.4 %reduce-scatter.13.cloned.1.call-done = bf16[128,1024]{1,0:T(8,128)(2,1)} async-done(((bf16[512,1024]{1,0:T(8,128)(2,1)}), bf16[128,1024]{1,0:T(8,128)(2,1)}) %reduce-scatter.13.cloned.1.call-update) | async-done | bytes 262160
  209.6 1.0 copy.47
  210.6 0.2 copy.36
  210.8 0.2 fusion.42
  211.1 5.8 %collective-permute-done = bf16[8,128,128]{2,1,0:T(8,128)(2,1)S(1)} collective-permute-done((bf16[8,128,128]{2,1,0:T(8,128)(2,1)S(1)}, bf16[8,128,128]{2,1,0:T(8,128)(2,1)S(1)}, u32[]{:S(2)}, u32[]{:S(2)}) %collective-permute-start) | collective-permute-done | bytes 262176 | tf_op jit(solution)/shard_map/ppermute | solution.py:17
  216.9 5.8 %collective-permute-done.1 = bf16[8,128,128]{2,1,0:T(8,128)(2,1)S(1)} collective-permute-done((bf16[8,128,128]{2,1,0:T(8,128)(2,1)S(1)}, bf16[8,128,128]{2,1,0:T(8,128)(2,1)S(1)}, u32[]{:S(2)}, u32[]{:S(2)}) %collective-permute-start.1) | collective-permute-done | bytes 262176 | tf_op jit(solution)/shard_map/ppermute | solution.py:17
  222.7 5.8 %collective-permute-done.2 = bf16[8,128,128]{2,1,0:T(8,128)(2,1)S(1)} collective-permute-done((bf16[8,128,128]{2,1,0:T(8,128)(2,1)S(1)}, bf16[8,128,128]{2,1,0:T(8,128)(2,1)S(1)}, u32[]{:S(2)}, u32[]{:S(2)}) %collective-permute-start.2) | collective-permute-done | bytes 262176 | tf_op jit(solution)/shard_map/ppermute | solution.py:17
  228.5 4.4 %convolution_convert_fusion.1 = bf16[8,128,1024]{2,1,0:T(8,128)(2,1)} fusion(s32[]{:T(128)S(6)} %select_n.44, bf16[8,128,128]{2,1,0:T(8,128)(2,1)S(1)} %collective-permute-done.2, bf16[8,128,128]{2,1,0:T(8,128)(2,1)S(1)} %collective-permute-done.1, bf16[8,128,128]{2,1,0:T(8,128)(2,1)S(1)} %collective-permute-done, bf16[8,128,128]{2,1,0:T(8,128)(2,1)S(1)} %fusion.42, ...), kind=kOutput, calls=%fused_computation.32 | convolution fusion | flops 1083179008 | bytes 4194308 | tf_op jit(solution)/shard_map/scf,fd->scd/dot_general | solution.py:39
  232.9 3.9 %all-to-all-done.3 = bf16[8,128,1024]{2,1,0:T(8,128)(2,1)S(1)} async-done(((bf16[8,128,1024]{2,1,0:T(8,128)(2,1)}), bf16[8,128,1024]{2,1,0:T(8,128)(2,1)S(1)}, u32[]{:S(2)}, u32[]{:S(2)}) %all-to-all-start.3) | async-done | bytes 2097184 | tf_op jit(solution)/shard_map/all_to_all | solution.py:45
  236.8 4.3 %all-to-all-start.1 = ((bf16[8,128,1024]{2,1,0:T(8,128)(2,1)}), bf16[8,128,1024]{2,1,0:T(8,128)(2,1)}, u32[]{:S(2)}, u32[]{:S(2)}) async-start(bf16[8,128,1024]{2,1,0:T(8,128)(2,1)} %convolution_convert_fusion.1), calls=%async_computation.1 | async-start | bytes 4194304 | tf_op jit(solution)/shard_map/all_to_all | solution.py:45
  241.2 0.3 fusion.43
  241.5 47.5 %all-to-all-done.1 = bf16[8,128,1024]{2,1,0:T(8,128)(2,1)} async-done(((bf16[8,128,1024]{2,1,0:T(8,128)(2,1)}), bf16[8,128,1024]{2,1,0:T(8,128)(2,1)}, u32[]{:S(2)}, u32[]{:S(2)}) %all-to-all-start.1) | async-done | bytes 2097184 | tf_op jit(solution)/shard_map/all_to_all | solution.py:45
  289.0 2.0 pad_maximum_fusion
  290.9 2.4 copy.34
  293.3 5.5 %gather_fusion.2 = bf16[512,1024]{1,0:T(8,128)(2,1)S(1)} fusion(bf16[2048,1024]{1,0:T(8,128)(2,1)} %bitcast.99, s32[1024]{0:T(1024)S(1)} %get-tuple-element.14), kind=kCustom, calls=%fused_computation.2 | custom fusion | bytes 2099200 | tf_op jit(solution)/shard_map/gather | solution.py:85
  298.8 5.5 %gather_fusion.1 = bf16[512,1024]{1,0:T(8,128)(2,1)S(1)} fusion(bf16[2048,1024]{1,0:T(8,128)(2,1)} %bitcast.100, s32[1024]{0:T(1024)S(1)} %get-tuple-element.15), kind=kCustom, calls=%fused_computation.1 | custom fusion | bytes 2099200 | tf_op jit(solution)/shard_map/gather | solution.py:85
  304.2 0.6 multiply_reduce_fusion
  304.9 5.7 %psum.15 = f32[512]{0:T(512)S(1)} all-reduce(f32[512]{0:T(512)S(1)} %multiply_reduce_fusion), channel_id=1, replica_groups=mesh['ep'=8,'tp'=4] {'tp'}, use_global_device_ids=true, to_apply=%region_11.13 | all-reduce | flops 512 | bytes 4096 | tf_op jit(solution)/shard_map/psum | solution.py:88
  310.6 1.6 multiply_convert_fusion
  (38 shorter events, 0.5 us)
Async XLA Ops:
  6.5 21.0 %copy-start = (bf16[512,1024]{1,0:T(8,128)(2,1)S(1)}, bf16[512,1024]{1,0:T(8,128)(2,1)}, u32[]{:S(2)}) copy-start(bf16[512,1024]{1,0:T(8,128)(2,1)} %param.10) | copy-start | bytes 3145732
  6.5 21.0 %copy-start.1 = (f32[1024]{0:T(1024)S(1)}, f32[1024]{0:T(1024)}, u32[]{:S(2)}) copy-start(f32[1024]{0:T(1024)} %param.13) | copy-start | bytes 12292
  6.5 149.8 %reduce-scatter.19.cloned.1.call-start = ((), (), s32[]{:S(2)}) async-start(), calls=%async_computation.11 | async-start | bytes 1310720
  41.6 52.7 %copy-start.4 = (bf16[2,1024,512]{2,1,0:T(8,128)(2,1)S(1)}, bf16[2,1024,512]{2,1,0:T(8,128)(2,1)}, u32[]{:S(2)}) copy-start(bf16[2,1024,512]{2,1,0:T(8,128)(2,1)} %param.15) | copy-start | bytes 6291460
  99.5 51.6 %all-to-all-start = ((bf16[8,128,1024]{2,1,0:T(8,128)(2,1)}), bf16[8,128,1024]{2,1,0:T(8,128)(2,1)}, u32[]{:S(2)}, u32[]{:S(2)}) async-start(bf16[8,128,1024]{2,1,0:T(8,128)(2,1)} %get-tuple-element.8), calls=%async_computation | async-start | bytes 4194304 | tf_op jit(solution)/shard_map/all_to_all | solution.py:77
  103.9 53.7 %reduce-scatter.17.cloned.1.call-start = ((), (), s32[]{:S(2)}) async-start(), calls=%async_computation.10 | async-start | bytes 1310720
  110.4 79.5 %reduce-scatter.15.cloned.1.call-start = ((), (), s32[]{:S(2)}) async-start(), calls=%async_computation.9 | async-start | bytes 1310720
  156.3 53.3 %reduce-scatter.13.cloned.1.call-start = ((), (), s32[]{:S(2)}) async-start(), calls=%async_computation.8 | async-start | bytes 1310720
  159.0 5.8 %collective-permute-start.3 = (bf16[8,128,128]{2,1,0:T(8,128)(2,1)S(1)}, bf16[8,128,128]{2,1,0:T(8,128)(2,1)S(1)}, u32[]{:S(2)}, u32[]{:S(2)}) collective-permute-start(bf16[8,128,128]{2,1,0:T(8,128)(2,1)S(1)} %fusion.41), channel_id=1, source_target_pairs={{0,1},{1,2},{2,3},{3,0},{4,5},{5,6},{6,7},{7,4},{8,9},{9,10},{10,1... | collective-permute-start | bytes 786440 | tf_op jit(solution)/shard_map/ppermute | solution.py:17
  164.9 5.8 %collective-permute-start.4 = (bf16[8,128,128]{2,1,0:T(8,128)(2,1)S(1)}, bf16[8,128,128]{2,1,0:T(8,128)(2,1)S(1)}, u32[]{:S(2)}, u32[]{:S(2)}) collective-permute-start(bf16[8,128,128]{2,1,0:T(8,128)(2,1)S(1)} %collective-permute-done.3), channel_id=1, source_target_pairs={{0,1},{1,2},{2,3},{3,0},{4,5},{5,6},{6,7},{7,4},{8,9},{9,10},{10,1... | collective-permute-start | bytes 786440 | tf_op jit(solution)/shard_map/ppermute | solution.py:17
  170.7 11.2 %collective-permute-start.5 = (bf16[8,128,128]{2,1,0:T(8,128)(2,1)S(1)}, bf16[8,128,128]{2,1,0:T(8,128)(2,1)S(1)}, u32[]{:S(2)}, u32[]{:S(2)}) collective-permute-start(bf16[8,128,128]{2,1,0:T(8,128)(2,1)S(1)} %collective-permute-done.4), channel_id=1, source_target_pairs={{0,1},{1,2},{2,3},{3,0},{4,5},{5,6},{6,7},{7,4},{8,9},{9,10},{10,1... | collective-permute-start | bytes 786440 | tf_op jit(solution)/shard_map/ppermute | solution.py:17
  186.3 50.5 %all-to-all-start.3 = ((bf16[8,128,1024]{2,1,0:T(8,128)(2,1)}), bf16[8,128,1024]{2,1,0:T(8,128)(2,1)S(1)}, u32[]{:S(2)}, u32[]{:S(2)}) async-start(bf16[8,128,1024]{2,1,0:T(8,128)(2,1)} %convolution_convert_fusion), calls=%async_computation.3 | async-start | bytes 4194304 | tf_op jit(solution)/shard_map/all_to_all | solution.py:45
  211.0 5.8 %collective-permute-start = (bf16[8,128,128]{2,1,0:T(8,128)(2,1)S(1)}, bf16[8,128,128]{2,1,0:T(8,128)(2,1)S(1)}, u32[]{:S(2)}, u32[]{:S(2)}) collective-permute-start(bf16[8,128,128]{2,1,0:T(8,128)(2,1)S(1)} %fusion.42), channel_id=1, source_target_pairs={{0,1},{1,2},{2,3},{3,0},{4,5},{5,6},{6,7},{7,4},{8,9},{9,10},{10,1... | collective-permute-start | bytes 786440 | tf_op jit(solution)/shard_map/ppermute | solution.py:17
  216.9 5.8 %collective-permute-start.1 = (bf16[8,128,128]{2,1,0:T(8,128)(2,1)S(1)}, bf16[8,128,128]{2,1,0:T(8,128)(2,1)S(1)}, u32[]{:S(2)}, u32[]{:S(2)}) collective-permute-start(bf16[8,128,128]{2,1,0:T(8,128)(2,1)S(1)} %collective-permute-done), channel_id=1, source_target_pairs={{0,1},{1,2},{2,3},{3,0},{4,5},{5,6},{6,7},{7,4},{8,9},{9,10},{10,1... | collective-permute-start | bytes 786440 | tf_op jit(solution)/shard_map/ppermute | solution.py:17
  222.7 5.8 %collective-permute-start.2 = (bf16[8,128,128]{2,1,0:T(8,128)(2,1)S(1)}, bf16[8,128,128]{2,1,0:T(8,128)(2,1)S(1)}, u32[]{:S(2)}, u32[]{:S(2)}) collective-permute-start(bf16[8,128,128]{2,1,0:T(8,128)(2,1)S(1)} %collective-permute-done.1), channel_id=1, source_target_pairs={{0,1},{1,2},{2,3},{3,0},{4,5},{5,6},{6,7},{7,4},{8,9},{9,10},{10,1... | collective-permute-start | bytes 786440 | tf_op jit(solution)/shard_map/ppermute | solution.py:17
  232.9 8.6 %copy-start.3 = (f32[512,2]{0,1:T(2,128)S(1)}, f32[512,2]{0,1:T(2,128)}, u32[]{:S(2)}) copy-start(f32[512,2]{0,1:T(2,128)} %param.12) | copy-start | bytes 12292
  236.8 52.2 %all-to-all-start.1 = ((bf16[8,128,1024]{2,1,0:T(8,128)(2,1)}), bf16[8,128,1024]{2,1,0:T(8,128)(2,1)}, u32[]{:S(2)}, u32[]{:S(2)}) async-start(bf16[8,128,1024]{2,1,0:T(8,128)(2,1)} %convolution_convert_fusion.1), calls=%async_computation.1 | async-start | bytes 4194304 | tf_op jit(solution)/shard_map/all_to_all | solution.py:45
  304.2 6.3 %copy-start.2 = (f32[1024]{0:T(1024)S(1)}, f32[1024]{0:T(1024)}, u32[]{:S(2)}) copy-start(f32[1024]{0:T(1024)} %param.17) | copy-start | bytes 12292
Sparse Core Ops, SparseCore 0:
  99.7 23.8 reduce-scatter.18
  126.1 24.8 reduce-scatter.16
  156.4 26.7 reduce-scatter.14
  185.6 23.9 reduce-scatter.12
